TPU v7x, 32 devices: a whole 2x2x4 slice. The times are simulated.
32 devices in a mesh: sp: 8 (over z, x), tp: 4 (over y, core).
Axes of the slice: x: 2, y: 2, z: 4, core: 2. Of those that a mesh axis runs over, the one named last changes fastest.
Arguments:
- stream: bfloat16 [1024, 2048], P('sp', 'tp'), may hold values from -6 to 6
- norm_gain: float32 [2048], replicated, may hold values from 0.1 to 1.9
- w_query: bfloat16 [2048, 1024], P('sp', 'tp'), may hold values from -0.75 to 0.75
- w_key: bfloat16 [2048, 256], P('sp', 'tp'), may hold values from -0.125 to 0.125
- w_value: bfloat16 [2048, 256], P('sp', 'tp'), may hold values from -0.125 to 0.125
- w_conv_in: bfloat16 [2048, 1024], P('sp', 'tp'), may hold values from -0.125 to 0.125
- w_conv_gate: bfloat16 [2048, 1024], P('sp', 'tp'), may hold values from -0.125 to 0.125
- conv_taps: float32 [3, 1024], P(None, 'tp'), may hold values from -3.5 to 3.5
- sb_bias: float32 [16], P('tp'), may hold values from -28 to -13
- w_out_attn: bfloat16 [1024, 2048], P('tp', 'sp'), may hold values from -0.5 to 0.5
- w_out_conv: bfloat16 [1024, 2048], P('tp', 'sp'), may hold values from -0.125 to 0.125
Outputs:
- mixed: bfloat16 [1024, 2048], P('sp', 'tp')
- log_weight_sum: float32 [16, 1024], P('tp', 'sp')
All inputs are finite; a program needn't handle non-finite values.
Results may differ from a plain program's by a relative error of at most 0.013.
The roundings to bfloat16 on the way count: a program that leaves them out, or rounds other values in their place, can miss the bound.
Values may be sent and summed in bfloat16 or wider, within the bound.
A program may use at most 64 MiB of HBM per device.

v0:
```python
import jax
import jax.numpy as jnp
from jax import lax
from jax.sharding import PartitionSpec as P

D = 2048
HEAD = 64
CONV_K = 3


EPS = 1e-06
FLOOR = 0.02


def from_behind(value, axis, steps):
    count = lax.axis_size(axis)
    leading, last = (max(0, -steps), min(count, count - steps))
    return lax.ppermute(value, axis, [(source, source + steps) for source in range(leading, last)])


def head_scores(query_head, key_rows, key_pos, query_pos, offset):
    scores = (
        jnp.einsum("qd,kd->qk", query_head, key_rows, preferred_element_type=jnp.float32)
        * HEAD ** (-0.5)
        + offset
    )
    causal = key_pos[None, :] < query_pos[:, None]
    fails = jnp.where(causal, jax.nn.log_sigmoid(-scores), 0.0)
    return (scores, causal, fails)


def split_heads(query):
    return [query[:, head * HEAD : (head + 1) * HEAD] for head in range(query.shape[1] // HEAD)]


def sweep_keys(all_keys, all_values, query, first, tokens, sb_bias):
    rows = query.shape[0]
    query_heads = split_heads(query)
    heads = len(query_heads)
    query_pos = first + jnp.arange(rows, dtype=jnp.int32)
    span = 8 * tokens
    spans = all_keys.shape[0] // span
    my_span = first // span

    def turn(step, carry):

        def work(state):
            outs, survs = state
            begin = (my_span - step) * span
            key_rows = lax.dynamic_slice_in_dim(all_keys, begin, span, 0)
            value_rows = lax.dynamic_slice_in_dim(all_values, begin, span, 0)
            key_pos = begin + jnp.arange(span, dtype=jnp.int32)
            added_outs = []
            added_survs = []
            for head in range(heads):
                scores, causal, fails = head_scores(
                    query_heads[head], key_rows, key_pos, query_pos, sb_bias[head]
                )
                later = lax.cumsum(fails, axis=1, reverse=True) - fails + survs[head][:, None]
                stick = jnp.where(causal, jnp.exp(jax.nn.log_sigmoid(scores) + later), 0.0).astype(
                    jnp.bfloat16
                )
                added_outs.append(
                    outs[head] + jnp.dot(stick, value_rows, preferred_element_type=jnp.float32)
                )
                added_survs.append(survs[head] + jnp.sum(fails, axis=1))
            return (jnp.stack(added_outs), jnp.stack(added_survs))

        return lax.cond(step <= my_span, work, lambda state: state, carry)

    start_state = (
        jnp.zeros((heads, rows, HEAD), jnp.float32),
        jnp.zeros((heads, rows), jnp.float32),
    )
    return lax.fori_loop(0, spans, turn, start_state)


def local(
    stream,
    norm_gain,
    w_query,
    w_key,
    w_value,
    w_conv_in,
    w_conv_gate,
    conv_taps,
    sb_bias,
    w_out_attn,
    w_out_conv,
):
    tokens = stream.shape[0]
    weights = (
        lax.all_gather(w_query, "sp", axis=0, tiled=True),
        lax.all_gather(w_key, "sp", axis=0, tiled=True),
        lax.all_gather(w_value, "sp", axis=0, tiled=True),
        lax.all_gather(w_conv_in, "sp", axis=0, tiled=True),
        lax.all_gather(w_conv_gate, "sp", axis=0, tiled=True),
    )
    piece_f = lax.all_gather(stream, "tp", axis=1, tiled=True).astype(jnp.float32)
    scaled = (piece_f * norm_gain[None, :]).astype(jnp.bfloat16)
    sums = tuple(
        (jnp.dot(scaled, weight, preferred_element_type=jnp.float32) for weight in weights)
    )
    sums, squares = (sums, jnp.sum(piece_f * piece_f, axis=1))
    row_scale = lax.rsqrt(squares / D + EPS)[:, None]
    query, keys, values, conv_in, conv_gate = [
        (total * row_scale).astype(jnp.bfloat16) for total in sums
    ]
    previous = from_behind(conv_in[tokens - (CONV_K - 1) :], "sp", 1)
    padded = jnp.concatenate([previous, conv_in], axis=0).astype(jnp.float32)
    conv_mixed = jnp.zeros((tokens, conv_in.shape[1]), jnp.float32)
    for tap in range(CONV_K):
        conv_mixed = conv_mixed + conv_taps[tap][None, :] * padded[tap : tap + tokens]
    conv_out = (conv_gate.astype(jnp.float32) * conv_mixed).astype(jnp.bfloat16)
    heads = query.shape[1] // HEAD
    my_index = lax.axis_index("sp")
    groups = [(query, my_index * tokens)]
    all_keys, all_values = (
        lax.all_gather(keys, "sp", axis=0, tiled=True),
        lax.all_gather(values, "sp", axis=0, tiled=True),
    )
    results = [
        sweep_keys(all_keys, all_values, rows_in, first, tokens, sb_bias)
        for rows_in, first in groups
    ]
    attended = results[0][0].astype(jnp.bfloat16)
    survs = results[0][1]
    log_weight_sum = jnp.log(jnp.maximum(-jnp.expm1(survs), FLOOR))
    attended_weight, conv_weight = (
        lax.all_gather(w_out_attn, "sp", axis=1, tiled=True),
        lax.all_gather(w_out_conv, "sp", axis=1, tiled=True),
    )
    partial_value = jnp.einsum(
        "hqd,hde->qe",
        attended,
        attended_weight.reshape(heads, HEAD, attended_weight.shape[1]),
        preferred_element_type=jnp.float32,
    )
    partial_value = partial_value + jnp.dot(
        conv_out, conv_weight, preferred_element_type=jnp.float32
    )
    mixed = lax.psum_scatter(
        partial_value.astype(jnp.bfloat16), "tp", scatter_dimension=1, tiled=True
    )
    return (mixed, log_weight_sum)


def solution(mesh):
    placed = (
        P("sp", "tp"),
        P(),
        P("sp", "tp"),
        P("sp", "tp"),
        P("sp", "tp"),
        P("sp", "tp"),
        P("sp", "tp"),
        P(None, "tp"),
        P("tp"),
        P("tp", "sp"),
        P("tp", "sp"),
    )
    return jax.shard_map(
        local, mesh=mesh, in_specs=placed, out_specs=(P("sp", "tp"), P("tp", "sp")), check_vma=False
    )
```

profile of v0, /device:TPU:25, one launch (start us, length us, event | category | flops | bytes accessed | tf_op | source)
XLA Modules:
  0.0 249.4 jit_solution(3962702125349767598)
XLA Ops:
  10.6 7.7 %all_gather.30 = bf16[128,2048]{1,0:T(8,128)(2,1)S(1)} all-gather(bf16[128,512]{1,0:T(8,128)(2,1)S(1)} %copy-done.4), channel_id=1, replica_groups=mesh['sp'=8,'tp'=4] {'tp'}, dimensions={1}, use_global_device_ids=true | all-gather | bytes 655360 | tf_op jit(solution)/shard_map/all_gather | solution.py:99
  19.3 23.1 %all_gather.34 = bf16[2048,64]{0,1:T(8,128)(2,1)S(1)} all-gather(bf16[256,64]{0,1:T(8,128)(2,1)S(1)} %copy-done.6), channel_id=1, replica_groups=mesh['sp'=8,'tp'=4] {'sp'}, dimensions={0}, use_global_device_ids=true | all-gather | bytes 294912 | tf_op jit(solution)/shard_map/all_gather | solution.py:95
  42.8 21.1 %all_gather.35 = bf16[1024,64]{0,1:T(8,128)(2,1)S(1)} all-gather(bf16[128,64]{0,1:T(8,128)(2,1)S(1)} %fusion.60), channel_id=1, replica_groups=mesh['sp'=8,'tp'=4] {'sp'}, dimensions={0}, use_global_device_ids=true | all-gather | bytes 147456 | tf_op jit(solution)/shard_map/all_gather | solution.py:120
  63.9 25.5 %all_gather.32 = bf16[2048,64]{0,1:T(8,128)(2,1)S(1)} all-gather(bf16[256,64]{0,1:T(8,128)(2,1)S(1)} %copy-done.7), channel_id=1, replica_groups=mesh['sp'=8,'tp'=4] {'sp'}, dimensions={0}, use_global_device_ids=true | all-gather | bytes 294912 | tf_op jit(solution)/shard_map/all_gather | solution.py:94
  89.8 21.5 %all_gather.33 = bf16[1024,64]{0,1:T(8,128)(2,1)S(1)} all-gather(bf16[128,64]{0,1:T(8,128)(2,1)S(1)} %fusion.59), channel_id=1, replica_groups=mesh['sp'=8,'tp'=4] {'sp'}, dimensions={0}, use_global_device_ids=true | all-gather | bytes 147456 | tf_op jit(solution)/shard_map/all_gather | solution.py:119
  111.9 1.5 fusion.58
  114.0 4.7 %collective-permute-start = (bf16[2,256]{1,0:T(2,128)(2,1)}, bf16[2,256]{1,0:T(2,128)(2,1)}, u32[]{:S(2)}, u32[]{:S(2)}) collective-permute-start(bf16[2,256]{1,0:T(2,128)(2,1)} %slice.124), channel_id=1, source_target_pairs={{0,4},{4,8},{8,12},{12,16},{16,20},{20,24},{24,28},{1,5},{5,9},{9,... | collective-permute-start | bytes 3080 | tf_op jit(solution)/shard_map/ppermute | solution.py:18
  118.8 1.5 fusion.53
  121.0 73.6 %conditional.1 = ((f32[4,128,64]{1,2,0:T(8,128)S(1)}, f32[4,128]{1,0:T(4,128)S(1)})) conditional(s32[]{:T(128)} %convert_element_type.58, (f32[4,128,64]{1,2,0:T(8,128)S(1)}, f32[4,128]{1,0:T(4,128)S(1)}) %tuple.31, (f32[4,128,64]{1,2,0:T(8,128)S(1)}, s32[]{:T(128)}, s32[]{:T(128)}, s32[128]{0:T(128)S(1)}, bf16[128,256]{1,0:T(8,128)(2,1)S(1)}, ...), branch_computations={%region_1.2_spmd, %region_2.15_spmd} | conditional | flops 218925184 | bytes 41723780 | solution.py:69
  121.6 0.8 fusion
  122.5 0.9 fusion.1
  123.4 0.8 fusion.2
  124.2 0.8 fusion.3
  125.1 2.3 fusion.44
  128.1 1.0 copy.14
  129.1 2.1 fusion.81
  131.3 0.8 broadcast_add_fusion.3
  132.1 2.1 copy.15
  134.2 2.0 fusion.7
  136.4 1.0 copy.16
  137.4 2.1 fusion.82
  139.6 0.8 broadcast_add_fusion.2
  140.4 1.3 copy.17
  142.3 0.9 fusion.6
  143.7 23.3 %fusion.83 = f32[128,8,128]{0,1,2:T(8,128)S(1)} fusion(f32[128,8,128]{0,1,2:T(8,128)S(1)} %copy.18), kind=kOutput, calls=%fused_computation.134 | output fusion | flops 16646144 | bytes 1048576 | tf_op jit(solution)/shard_map/reduce-window.4
  168.0 0.9 fusion.5
  169.3 23.3 %fusion.84 = f32[128,8,128]{0,1,2:T(8,128)S(1)} fusion(f32[128,8,128]{0,1,2:T(8,128)S(1)} %copy.20), kind=kOutput, calls=%fused_computation.135 | output fusion | flops 16646144 | bytes 1048576 | tf_op jit(solution)/shard_map/reduce-window.6
  193.6 0.9 fusion.4
  194.6 1.6 convolution_bitcast_fusion
  196.9 17.5 %all-gather.14.cloned.1.call-done = bf16[256,2048]{1,0:T(8,128)(2,1)} async-done(((bf16[256,256]{1,0:T(8,128)(2,1)}), bf16[256,2048]{1,0:T(8,128)(2,1)}) %all-gather.14.cloned.1.call-update) | async-done | bytes 1048592 | tf_op jit(solution)/shard_map/all_gather | solution.py:131
  215.1 3.1 %fusion.52 = bf16[128,2048]{1,0:T(8,128)(2,1)} fusion(f32[128,2048]{1,0:T(8,128)S(1)} %convolution_bitcast_fusion, bf16[256,2048]{1,0:T(8,128)(2,1)} %all-gather.14.cloned.1.call-done, bf16[2048,256]{1,0:T(8,128)(2,1)} %all-gather.10.cloned.1.call-done, bf16[128,2048]{1,0:T(8,128)(2,1)S(1)} %all_gather.30, f32[2048]{0:T(1024)S(1)} %copy-done.5, ...), kind=kOutput, calls=%fused_computation.98 | convolution fusion | flops 270073856 | bytes 4599296 | tf_op jit(solution)/shard_map/dot_general | solution.py:139
  218.8 23.7 %reduce-scatter.2.cloned.1.call-done = bf16[128,512]{1,0:T(8,128)(2,1)} async-done(((bf16[128,2048]{1,0:T(8,128)(2,1)}), bf16[128,512]{1,0:T(8,128)(2,1)}) %reduce-scatter.2.cloned.1.call-update) | async-done | bytes 131088 | tf_op jit(solution)/shard_map/reduce_scatter | solution.py:142
  (98 shorter events, 13.7 us)
Async XLA Ops:
  7.2 104.7 %all-gather.12.cloned.1.call-start = ((), (), s32[]{:S(2)}) async-start(), calls=%async_computation.4 | async-start | bytes 1179648 | tf_op jit(solution)/shard_map/all_gather | solution.py:96
  7.9 110.8 %all-gather.6.cloned.1.call-start = ((), (), s32[]{:S(2)}) async-start(), calls=%async_computation.1 | async-start | bytes 1179648 | tf_op jit(solution)/shard_map/all_gather | solution.py:93
  8.6 185.9 %all-gather.8.cloned.1.call-start = ((), (), s32[]{:S(2)}) async-start(), calls=%async_computation.2 | async-start | bytes 1179648 | tf_op jit(solution)/shard_map/all_gather | solution.py:130
  9.4 1.2 copy-start.4
  9.4 187.5 %all-gather.10.cloned.1.call-start = ((), (), s32[]{:S(2)}) async-start(), calls=%async_computation.3 | async-start | bytes 1179648 | tf_op jit(solution)/shard_map/all_gather | solution.py:97
  10.0 204.4 %all-gather.14.cloned.1.call-start = ((), (), s32[]{:S(2)}) async-start(), calls=%async_computation.5 | async-start | bytes 1179648 | tf_op jit(solution)/shard_map/all_gather | solution.py:131
  10.6 232.0 %reduce-scatter.2.cloned.1.call-start = ((), (), s32[]{:S(2)}) async-start(), calls=%async_computation.6 | async-start | bytes 655360 | tf_op jit(solution)/shard_map/reduce_scatter | solution.py:142
  18.5 100.2 %copy-start.9 = (f32[128]{0:T(128)}, f32[128]{0:T(128)S(1)}, u32[]{:S(2)}) copy-start(f32[128]{0:T(128)S(1)} %add_rsqrt_fusion) | copy-start | bytes 1540
  18.6 0.8 copy-start.6
  19.3 23.1 %copy-start.5 = (f32[2048]{0:T(1024)S(1)}, f32[2048]{0:T(1024)}, u32[]{:S(2)}) copy-start(f32[2048]{0:T(1024)} %param.14) | copy-start | bytes 24580
  42.8 21.2 %copy-start.7 = (bf16[256,64]{0,1:T(8,128)(2,1)S(1)}, bf16[256,64]{0,1:T(8,128)(2,1)}, u32[]{:S(2)}) copy-start(bf16[256,64]{0,1:T(8,128)(2,1)} %param.16) | copy-start | bytes 98308
  89.8 21.5 %copy-start.14 = (f32[3,256]{1,0:T(4,128)S(1)}, f32[3,256]{1,0:T(4,128)}, u32[]{:S(2)}) copy-start(f32[3,256]{1,0:T(4,128)} %param.20) | copy-start | bytes 9220
  114.0 82.1 %collective-permute-start = (bf16[2,256]{1,0:T(2,128)(2,1)}, bf16[2,256]{1,0:T(2,128)(2,1)}, u32[]{:S(2)}, u32[]{:S(2)}) collective-permute-start(bf16[2,256]{1,0:T(2,128)(2,1)} %slice.124), channel_id=1, source_target_pairs={{0,4},{4,8},{8,12},{12,16},{16,20},{20,24},{24,28},{1,5},{5,9},{9,... | collective-permute-start | bytes 3080 | tf_op jit(solution)/shard_map/ppermute | solution.py:18
  120.3 0.7 copy-start.8
  122.5 2.6 %copy-start.1 = (f32[128,1024]{1,0:T(8,128)}, f32[128,1024]{1,0:T(8,128)S(1)}, u32[]{:S(2)}) copy-start(f32[128,1024]{1,0:T(8,128)S(1)} %fusion) | copy-start | bytes 1572868 | tf_op jit(solution)/shard_map/while/body/eval_jaxpr/cond
  125.1 9.2 %copy-start.15 = (s32[128]{0:T(128)}, s32[128]{0:T(128)S(1)}, u32[]{:S(2)}) copy-start(s32[128]{0:T(128)S(1)} %broadcast_add_fusion.4) | copy-start | bytes 1540 | tf_op jit(solution)/shard_map/while/body/eval_jaxpr/cond
  132.1 2.1 copy-start.2
  134.2 2.0 copy-start.3
  141.7 0.6 copy-start.16
  141.7 0.6 copy-start.20
  142.3 1.0 copy-start
  167.4 0.6 copy-start.17
  167.4 0.6 copy-start.19
  193.0 0.6 copy-start.18
  194.5 19.9 %copy-start.12 = (f32[1,256]{1,0:T(1,128)S(1)}, f32[1,256]{1,0:T(1,128)}, u32[]{:S(2)}) copy-start(f32[1,256]{1,0:T(1,128)} %get-tuple-element.136) | copy-start | bytes 3076
  194.6 19.9 %copy-start.13 = (f32[1,256]{1,0:T(1,128)S(1)}, f32[1,256]{1,0:T(1,128)}, u32[]{:S(2)}) copy-start(f32[1,256]{1,0:T(1,128)} %get-tuple-element.137) | copy-start | bytes 3076
  214.4 0.6 copy-start.10
  214.4 0.7 copy-start.11
Sparse Core Ops, SparseCore 0:
  10.1 39.2 all-gather.11
  51.5 40.7 all-gather.5
  94.4 38.5 all-gather.7
  135.0 39.5 all-gather.9
  176.5 37.8 all-gather.13
  218.4 24.1 reduce-scatter.1
where the time goes:
time: 252 us; the launch traced here: 249 us
  blocking collectives  99 us (39%)
  other arithmetic  57.1 us (23%)
  waiting for transfers between devices  44.4 us (18%)
  matrix products  16.4 us (7%)
  between operations  14.3 us (6%)
  local copies, waits for them, and re-layouts  12.9 us (5%)
  starting transfers between devices  4.94 us (2%)
    another operation x8, other arithmetic  50.9 us
    all_gather x1, blocking collectives, local(): lax.all_gather(w_key, 'sp', axis=0, tiled=True)  25.5 us
    reduce_scatter x1, waiting for transfers between devices, local(): lax.psum_scatter(partial_value.astype(jnp.bfloat16), 'tp', scatter_dimens...  23.7 us
    all_gather x1, blocking collectives, local(): lax.all_gather(w_value, 'sp', axis=0, tiled=True)  23.1 us
    all_gather x1, blocking collectives, local(): lax.all_gather(keys, 'sp', axis=0, tiled=True)  21.5 us
    all_gather x1, blocking collectives, local(): lax.all_gather(values, 'sp', axis=0, tiled=True)  21.1 us
    all_gather x1, waiting for transfers between devices, local(): lax.all_gather(w_out_conv, 'sp', axis=1, tiled=True)  17.5 us
    all_gather x1, blocking collectives, local(): lax.all_gather(stream, 'tp', axis=1, tiled=True).astype(jnp.float32)  7.71 us
  transfers between devices with their start and end apart: 7, of which 2 were waited for; matrix products, arithmetic and copies ran while one was open for 32% of the time, Pallas kernels for 0%

commit v1 on v0

v1 whole, which is shorter than its diff:
```python
import functools

import jax
import jax.numpy as jnp
from jax import lax
from jax.experimental import pallas as pl
from jax.experimental.pallas import tpu as pltpu
from jax.sharding import PartitionSpec as P

HEAD = 64
CONV_K = 3
EPS = 1e-06
FLOOR = 0.02
MESH = pl.DeviceIdType.MESH
F32 = jnp.float32
BF16 = jnp.bfloat16


def kernel(n, groups, inner, heads,
           bias_ref, stream_ref, gain_ref, taps_ref, wq_ref, wci_ref, wcg_ref, wkv_ref, woa_ref, woc_ref,
           out_ref, lws_ref,
           xbuf, scaled, wbuf, wobuf, kvbuf, qbuf, gate, cin, halo, mix, carry, acc, pbuf, rbuf,
           lsem, xsend, xrecv, wup, wdn, wx, wrecv, oup, odn, ox, orecv, ksend, krecv, hsem, psend, precv):
    me, tp = lax.axis_index("sp"), lax.axis_index("tp")
    outer = n // inner
    o, i = me // inner, lax.rem(me, inner)
    rows, tokens = wq_ref.shape[0], stream_ref.shape[0]
    features = stream_ref.shape[1]
    width = wq_ref.shape[1]
    conv = wci_ref.shape[1]
    arows = woa_ref.shape[0]
    per = n // groups

    def wrows(block):
        return pl.ds(pl.multiple_of(block * rows, rows), rows)

    own = wbuf.at[wrows(me)]
    local = [
        (wq_ref, own.at[:, 0:width]),
        (wci_ref, own.at[:, width:width + conv]),
        (wcg_ref, own.at[:, width + conv:width + 2 * conv]),
        (wkv_ref, own.at[:, width + 2 * conv:width + 2 * conv + 2 * HEAD]),
        (stream_ref, xbuf.at[tp]),
        (woa_ref, wobuf.at[me, 0:arows]),
        (woc_ref, wobuf.at[me, arows:2 * arows]),
    ]
    local = [pltpu.make_async_copy(src, dst, lsem.at[j]) for j, (src, dst) in enumerate(local)]
    for copy in local:
        copy.start()

    barrier = pltpu.get_barrier_semaphore()

    def greet(d, _):
        pl.semaphore_signal(barrier, inc=1, device_id={"sp": lax.rem(me + d, n)}, device_id_type=MESH)
        return 0

    lax.fori_loop(1, n, greet, 0)
    for d in range(1, groups):
        pl.semaphore_signal(barrier, inc=1, device_id={"tp": lax.rem(tp + d, groups)}, device_id_type=MESH)
    pl.semaphore_wait(barrier, n - 1 + groups - 1)

    def relay_set(view, up, dn, xs, recv):
        def to(block, sem, oo, ii):
            return pltpu.make_async_remote_copy(
                src_ref=view(block), dst_ref=view(block), send_sem=sem.at[block], recv_sem=recv.at[block],
                device_id={"sp": oo * inner + ii}, device_id_type=MESH)

        def at(oo):
            return oo * inner + i

        def x_each(f):
            for d in range(1, inner):
                f(d)

        def start_up(block):
            @pl.when(o < outer - 1)
            def _():
                to(block, up, o + 1, i).start()

        def start_dn(block):
            @pl.when(o > 0)
            def _():
                to(block, dn, o - 1, i).start()

        def start_x(block):
            x_each(lambda d: to(block, xs.at[d - 1], o, lax.rem(i + d, inner)).start())

        def begin():
            start_up(me)
            start_dn(me)
            start_x(me)

        def step(k):
            @pl.when(o - k >= 0)
            def _():
                block = at(o - k)
                to(block, up, o, i).wait_recv()
                start_up(block)
                start_x(block)

            @pl.when(o + k < outer)
            def _():
                block = at(o + k)
                to(block, dn, o, i).wait_recv()
                start_dn(block)
                start_x(block)

        def finish():
            def each(oo, _):
                block = at(oo)
                x_each(lambda d: to(block, xs.at[d - 1], o, i).wait_send())
                x_each(lambda d: to(oo * inner + lax.rem(i + d, inner), up, o, i).wait_recv())

                @pl.when(jnp.logical_and(oo <= o, o < outer - 1))
                def _():
                    to(block, up, o, i).wait_send()

                @pl.when(jnp.logical_and(oo >= o, o > 0))
                def _():
                    to(block, dn, o, i).wait_send()
                return 0

            lax.fori_loop(0, outer, each, 0)

        return begin, step, finish

    w_begin, w_step, w_finish = relay_set(lambda b: wbuf.at[wrows(b)], wup, wdn, wx, wrecv)
    o_begin, o_step, o_finish = relay_set(lambda b: wobuf.at[b], oup, odn, ox, orecv)

    def steps(step, first, last):
        lax.fori_loop(first, last, lambda k, c: (step(k), c)[1], 0)

    for copy in local:
        copy.wait()
    w_begin()

    def xcopy(source, target, d):
        return pltpu.make_async_remote_copy(
            src_ref=xbuf.at[source], dst_ref=xbuf.at[source], send_sem=xsend.at[d - 1], recv_sem=xrecv.at[d - 1],
            device_id={"tp": target}, device_id_type=MESH)

    for d in range(1, groups):
        xcopy(tp, lax.rem(tp + d, groups), d).start()
    for d in range(1, groups):
        xcopy(lax.rem(tp - d + groups, groups), tp, d).wait_recv()
    squares = jnp.zeros((tokens, 1), F32)
    for t in range(groups):
        part = xbuf[t].astype(F32)
        squares = squares + jnp.sum(part * part, axis=1, keepdims=True)
        cols = slice(t * features, (t + 1) * features)
        scaled[:, cols] = (part * gain_ref[:, cols]).astype(BF16)
    row_scale = lax.rsqrt(squares / (groups * features) + EPS)

    steps(w_step, 1, outer)
    o_begin()
    w_finish()

    def project(first, size):
        total = jnp.dot(scaled[...], wbuf[:, first:first + size], preferred_element_type=F32)
        return (total * row_scale).astype(BF16)

    kvbuf[me] = project(width + 2 * conv, 2 * HEAD)
    cin[...] = project(width, conv)
    query = project(0, width)
    for head in range(heads):
        piece = query[:, head * HEAD:(head + 1) * HEAD]
        qbuf[head] = jnp.concatenate([piece, jnp.zeros_like(piece)], axis=1)

    def kvcopy(block, target, slot):
        return pltpu.make_async_remote_copy(
            src_ref=kvbuf.at[block], dst_ref=kvbuf.at[block], send_sem=ksend.at[slot], recv_sem=krecv.at[block],
            device_id={"sp": target}, device_id_type=MESH)

    def hcopy(target):
        return pltpu.make_async_remote_copy(
            src_ref=cin.at[pl.ds(tokens - 16, 16)], dst_ref=halo, send_sem=hsem.at[0], recv_sem=hsem.at[1],
            device_id={"sp": target}, device_id_type=MESH)

    def push(target, _):
        kvcopy(me, target, target).start()
        return 0

    lax.fori_loop(me + 1, n, push, 0)

    @pl.when(me < n - 1)
    def _():
        hcopy(me + 1).start()

    gate[...] = project(width + conv, conv)
    steps(o_step, 1, min(2, outer))

    row_id = lax.broadcasted_iota(jnp.int32, (tokens, tokens), 0)
    col_id = lax.broadcasted_iota(jnp.int32, (tokens, tokens), 1)
    after = jnp.where(row_id > col_id, 1.0, 0.0).astype(BF16)
    sums = jnp.concatenate([after, jnp.ones_like(after)], axis=1)

    def attend(block, diagonal):
        pair = kvbuf[block]
        for head in range(heads):
            score = lax.dot_general(qbuf[head], pair, (((1,), (1,)), ((), ())), preferred_element_type=F32)
            score = score * HEAD ** (-0.5) + bias_ref[head]
            soft = jnp.log1p(jnp.exp(-jnp.abs(score)))
            fails = -jnp.maximum(score, 0.0) - soft
            if diagonal:
                fails = jnp.where(col_id < row_id, fails, 0.0)
            high = fails.astype(BF16)
            low = (fails - high.astype(F32)).astype(BF16)
            both = jnp.dot(high, sums, preferred_element_type=F32) + jnp.dot(low, sums, preferred_element_type=F32)
            later = both[:, :tokens]
            if not diagonal:
                later = later + carry[head]
            stick = jnp.exp(jnp.minimum(score, 0.0) - soft + later)
            if diagonal:
                stick = jnp.where(col_id < row_id, stick, 0.0)
            added = jnp.dot(stick.astype(BF16), pair, preferred_element_type=F32)
            if diagonal:
                carry[head] = both[:, tokens:]
                acc[head] = added
            else:
                carry[head] += both[:, tokens:]
                acc[head] += added

    attend(me, True)

    def turn(k, _):
        block = me - k
        kvcopy(block, me, 0).wait_recv()
        attend(block, False)
        return 0

    half = (me + 2) // 2
    lax.fori_loop(1, half, turn, 0)
    steps(o_step, 2, max(2, outer // 2 + 1))
    lax.fori_loop(half, me + 1, turn, 0)
    steps(o_step, max(2, outer // 2 + 1), outer)

    for pair in range(heads // 2):
        mix[:, pair * 2 * HEAD:(pair + 1) * 2 * HEAD] = jnp.concatenate(
            [acc[2 * pair][:, HEAD:], acc[2 * pair + 1][:, HEAD:]], axis=1).astype(BF16)
    for head in range(heads):
        survival = jnp.transpose(carry[head])[0:1, :]
        lws_ref[head:head + 1, :] = jnp.log(jnp.maximum(1.0 - jnp.exp(survival), FLOOR))

    @pl.when(me == 0)
    def _():
        halo[...] = jnp.zeros_like(halo)

    @pl.when(me > 0)
    def _():
        hcopy(me).wait_recv()

    padded = jnp.concatenate([halo[...].astype(F32), cin[...].astype(F32)], axis=0)
    mixed = jnp.zeros((tokens, conv), F32)
    for tap in range(CONV_K):
        begin = 16 - (CONV_K - 1) + tap
        mixed = mixed + taps_ref[tap:tap + 1, :] * padded[begin:begin + tokens]
    mix[:, heads * HEAD:] = (gate[...].astype(F32) * mixed).astype(BF16)

    o_finish()

    def partial(target):
        def one(b, _):
            block = target * per + b
            pbuf[block] = jnp.dot(mix[...], wobuf[block], preferred_element_type=F32).astype(BF16)
            return 0

        lax.fori_loop(0, per, one, 0)

    def pcopy(target, d):
        return pltpu.make_async_remote_copy(
            src_ref=pbuf.at[pl.ds(target * per, per)], dst_ref=rbuf.at[d - 1],
            send_sem=psend.at[d - 1], recv_sem=precv.at[d - 1],
            device_id={"tp": target}, device_id_type=MESH)

    for d in (2, 1, 3) if groups == 4 else range(1, groups):
        target = lax.rem(tp + d, groups)
        partial(target)
        pcopy(target, d).start()
    partial(tp)
    for d in range(1, groups):
        pcopy(tp, d).wait_recv()

    def total(b, _):
        value = pbuf[tp * per + b].astype(F32)
        for d in range(1, groups):
            value = value + rbuf[d - 1, b].astype(F32)
        out_ref[b] = value.astype(BF16)
        return 0

    lax.fori_loop(0, per, total, 0)

    for d in range(1, groups):
        pcopy(tp, d).wait_send()
        xcopy(tp, tp, d).wait_send()

    def pushed(target, _):
        kvcopy(me, me, target).wait_send()
        return 0

    lax.fori_loop(me + 1, n, pushed, 0)

    @pl.when(me < n - 1)
    def _():
        hcopy(me).wait_send()


def local(n, groups, stream, norm_gain, w_query, w_key, w_value, w_conv_in, w_conv_gate, conv_taps, sb_bias,
          w_out_attn, w_out_conv):
    tokens, features = stream.shape
    rows, width = w_query.shape
    conv = w_conv_in.shape[1]
    heads = width // HEAD
    arows, cols = w_out_attn.shape
    inner = 2 if n % 2 == 0 else 1
    per = n // groups
    w_kv = jnp.concatenate([w_key, w_value], axis=1)
    anywhere = pl.BlockSpec(memory_space=pl.ANY)
    vmem = pl.BlockSpec(memory_space=pltpu.VMEM)
    smem = pl.BlockSpec(memory_space=pltpu.SMEM)
    dma = pltpu.SemaphoreType.DMA
    out, lws = pl.pallas_call(
        functools.partial(kernel, n, groups, inner, heads),
        out_shape=(jax.ShapeDtypeStruct((per, tokens, cols), BF16), jax.ShapeDtypeStruct((heads, tokens), F32)),
        in_specs=[smem, anywhere, vmem, vmem] + [anywhere] * 6,
        out_specs=(vmem, vmem),
        scratch_shapes=[
            pltpu.VMEM((groups, tokens, features), BF16),
            pltpu.VMEM((tokens, groups * features), BF16),
            pltpu.VMEM((n * rows, width + 2 * conv + 2 * HEAD), BF16),
            pltpu.VMEM((n, 2 * arows, cols), BF16),
            pltpu.VMEM((n, tokens, 2 * HEAD), BF16),
            pltpu.VMEM((heads, tokens, 2 * HEAD), BF16),
            pltpu.VMEM((tokens, conv), BF16),
            pltpu.VMEM((tokens, conv), BF16),
            pltpu.VMEM((16, conv), BF16),
            pltpu.VMEM((tokens, width + conv), BF16),
            pltpu.VMEM((heads, tokens, tokens), F32),
            pltpu.VMEM((heads, tokens, 2 * HEAD), F32),
            pltpu.VMEM((n, tokens, cols), BF16),
            pltpu.VMEM((groups - 1, per, tokens, cols), BF16),
            dma((7,)),
            dma((groups - 1,)), dma((groups - 1,)),
            dma((n,)), dma((n,)), dma((max(1, inner - 1), n)), dma((n,)),
            dma((n,)), dma((n,)), dma((max(1, inner - 1), n)), dma((n,)),
            dma((n,)), dma((n,)),
            dma((2,)),
            dma((groups - 1,)), dma((groups - 1,)),
        ],
        compiler_params=pltpu.CompilerParams(
            collective_id=0, has_side_effects=True, vmem_limit_bytes=60 * 1024 * 1024
        ),
        name="layer",
    )(sb_bias, stream, norm_gain[None, :], conv_taps, w_query, w_conv_in, w_conv_gate, w_kv, w_out_attn, w_out_conv)
    return out.transpose(1, 0, 2).reshape(tokens, per * cols), lws


def solution(mesh):
    placed = (
        P("sp", "tp"),
        P(),
        P("sp", "tp"),
        P("sp", "tp"),
        P("sp", "tp"),
        P("sp", "tp"),
        P("sp", "tp"),
        P(None, "tp"),
        P("tp"),
        P("tp", "sp"),
        P("tp", "sp"),
    )
    body = functools.partial(local, mesh.shape["sp"], mesh.shape["tp"])
    return jax.shard_map(
        body, mesh=mesh, in_specs=placed, out_specs=(P("sp", "tp"), P("tp", "sp")), check_vma=False
    )
```

time: 252 us -> 87.7 us (0.35)
  blocking collectives: 99 us -> 0 us
  Pallas kernels: 0 us -> 82.7 us
  other arithmetic: 57.1 us -> 0.73 us
  waiting for transfers between devices: 44.4 us -> 0 us
  matrix products: 16.4 us -> 0 us
  between operations: 14.3 us -> 0.68 us
  local copies, waits for them, and re-layouts: 12.9 us -> 3.37 us
  starting transfers between devices: 4.94 us -> 0 us
    all_gather x5 -> x0, blocking collectives: 99 us -> none  [the longest x1 25.5 us: local(): lax.all_gather(w_key, 'sp', axis=0, tiled=True)]
    pallas_call x0 -> x1, Pallas kernels: none -> 82.7 us  [local(): pl.pallas_call(functools.partial(kernel, n, groups, inner, heads), out_sh...]
    another operation x14 -> x0, other arithmetic: 52.7 us -> none
    reduce_scatter x1 -> x0, waiting for transfers between devices: 23.7 us -> none  [local(): lax.psum_scatter(partial_value.astype(jnp.bfloat16), 'tp', scatter_dimens...]
    all_gather x5 -> x0, waiting for transfers between devices: 17.6 us -> none  [the longest x1 17.5 us: local(): lax.all_gather(w_out_conv, 'sp', axis=1, tiled=True)]
    dot_general x14 -> x0, matrix products: 16.4 us -> none  [the longest x4 4.66 us: work(): jnp.dot(stick, value_rows, preferred_element_type=jnp.float32)]
    another operation x15 -> x0, local copies, waits for them, and re-layouts: 5.53 us -> none  [the longest x4 3.92 us: work(): lax.cumsum(fails, axis=1, reverse=True) - fails + survs[head][:, None]]
    ppermute x1 -> x0, starting transfers between devices: 4.71 us -> none  [from_behind(): lax.ppermute(value, axis, [(source, source + steps) for source in range(l...]
  transfers between devices with their start and end apart: 7 -> 0, of which waited for: 2 -> 0; matrix products, arithmetic and copies ran while one was open for 32% -> 0% of each run, Pallas kernels for 0% -> 0%
where the time goes in v1:
time: 87.7 us; the launch traced here: 87.4 us
  Pallas kernels  82.7 us (94%)
  local copies, waits for them, and re-layouts  3.37 us (4%)
    pallas_call x1, Pallas kernels, local(): pl.pallas_call(functools.partial(kernel, n, groups, inner, heads), out_sh...  82.7 us
    unnamed x8, local copies, waits for them, and re-layouts  2.35 us

profile of v1, /device:TPU:25, one launch (start us, length us, event | category | flops | bytes accessed | tf_op | source)
XLA Modules:
  0.0 87.4 jit_solution(17997308153636568182)
XLA Ops:
  0.6 0.0 copy-start
  0.6 0.9 %copy.15 = bf16[256,64]{1,0:T(8,128)(2,1)S(1)} copy(bf16[256,64]{0,1:T(8,128)(2,1)} %param.14) | data formatting | bytes 65536 | tf_op args[3]
  1.5 0.0 copy-done
  1.5 0.1 copy.16
  1.6 0.7 pad_maximum_fusion.wkv_ref
  2.4 82.7 %layer.1 = (bf16[2,128,256]{2,1,0:T(8,128)(2,1)}, f32[4,128]{1,0:T(4,128)}) custom-call(f32[4]{0:T(128)} %bias_ref.1, bf16[128,512]{1,0:T(8,128)(2,1)} %stream_ref.1, f32[1,2048]{1,0:T(1,128)} %bitcast.5, f32[3,256]{1,0:T(4,128)} %taps_ref.1, bf16[256,256]{1,0:T(8,128)(2,1)} %wq_ref.1, bf16[256,256]{1,0:T(8,128)(2,1)} %wci_ref.1, bf16[256,256]{1,0:T(8,128)(2,1)} %wcg_ref.1, ...), custom_call_target="tpu_custom_call" | custom-call | tf_op jit(solution)/shard_map/layer/pallas_call | solution.py:321
  85.0 1.0 %copy.17 = bf16[128,2,256]{0,2,1:T(8,128)(2,1)S(1)} copy(bf16[128,2,256]{2,0,1:T(8,128)(2,1)} %bitcast.4) | data formatting | bytes 262144 | tf_op jit(solution)/shard_map/transpose | solution.py:354
  86.1 0.0 copy-start.1
  86.1 0.8 copy.18
  86.9 0.0 copy-done.1
  86.9 0.6 copy.20
Async XLA Ops:
  0.6 0.9 %copy-start = (bf16[256,64]{0,1:T(8,128)(2,1)S(1)}, bf16[256,64]{0,1:T(8,128)(2,1)}, u32[]{:S(2)}) copy-start(bf16[256,64]{0,1:T(8,128)(2,1)} %param.15) | copy-start | bytes 98308
  86.1 0.8 copy-start.1
